TPU v7x, 32 devices: a whole 2x2x4 slice. The times are simulated.
32 devices in a mesh: sp: 8 (over z, x), tp: 4 (over y, core).
Axes of the slice: x: 2, y: 2, z: 4, core: 2. Of those that a mesh axis runs over, the one named last changes fastest.
Arguments:
- hidden_in: bfloat16 [2048, 2048], P('sp'), may hold values from -6 to 6
- cotangent: bfloat16 [2048, 2048], P('sp'), may hold values from -6 to 6
- routes: int32 [2048, 2], P('sp'), may hold values from 0 to 7, all different within a row; in each aligned block of 256 rows (0 to 255, 256 to 511, ...) at most 96 rows name the same one
- routing_weights: float32 [2048, 2], P('sp'), may hold values from 0.1 to 1
- w_gate: bfloat16 [8, 2048, 1024], P('sp', None, 'tp'), may hold values from -0.125 to 0.125
- w_up: bfloat16 [8, 2048, 1024], P('sp', None, 'tp'), may hold values from -0.125 to 0.125
- w_down: bfloat16 [8, 1024, 2048], P('sp', 'tp'), may hold values from -0.1875 to 0.1875
- b_gate: bfloat16 [2048, 1024], P('sp', 'tp'), may hold values from -6 to 6
- c_gate: bfloat16 [2048, 1024], P('sp', 'tp'), may hold values from -6 to 6
- x_in: bfloat16 [2048, 1024], P('sp', 'tp'), may hold values from -6 to 6
- taps: bfloat16 [3, 1024], P(None, 'tp'), may hold values from -3 to 3
- w_out: bfloat16 [2048, 1024], P(None, 'tp'), may hold values from -0.1875 to 0.1875
Outputs:
- grad_gate: bfloat16 [8, 2048, 1024], P('sp', None, 'tp')
- grad_up: bfloat16 [8, 2048, 1024], P('sp', None, 'tp')
- grad_down: bfloat16 [8, 1024, 2048], P('sp', 'tp')
- out_proj_grad: float32 [2048, 1024], P('sp', 'tp')
- residual_grad: bfloat16 [2048, 2048], P('sp', 'tp')
- grad_b: bfloat16 [2048, 1024], P('sp', 'tp')
- grad_c: bfloat16 [2048, 1024], P('sp', 'tp')
- grad_x: bfloat16 [2048, 1024], P('sp', 'tp')
Inputs may be any that keep to these rules, and one draw needn't show every extreme that they name: `routes`: each row names 2 different experts. Among the rows of one index of sp no expert is named more than 96 times, a bound that some block reaches in some of them.
All inputs are finite; a program needn't handle non-finite values.
Results may differ from a plain program's by a relative error of at most 0.01.
Values may be sent and summed in bfloat16 or wider, within the bound.
A program may use at most 64 MiB of HBM per device.

v0:
```python
import jax
import jax.numpy as jnp
from jax import lax
from jax.sharding import PartitionSpec as P


def from_behind(x, axis, by):
    devices = lax.axis_size(axis)
    pairs = [(i, i + by) for i in range(devices) if 0 <= i + by < devices]
    return lax.ppermute(x, axis, pairs)


def per_device(
    hidden_in,
    cotangent,
    routes,
    routing_weights,
    w_gate,
    w_up,
    w_down,
    b_gate,
    c_gate,
    x_in,
    taps,
    w_out,
):
    tok_rows, model_width = hidden_in.shape
    top_k = routes.shape[1]
    local_experts = w_gate.shape[0]
    sp_size = lax.axis_size("sp")
    tp_size = lax.axis_size("tp")
    experts = local_experts * sp_size
    capacity = 3 * tok_rows * top_k // (2 * experts)
    slot_count = tok_rows * top_k
    feature_share = model_width // tp_size
    share_offset = lax.axis_index("tp") * feature_share
    flat_ids = routes.reshape(-1)
    onehot = (flat_ids[:, None] == jnp.arange(experts, dtype=jnp.int32)[None, :]).astype(jnp.int32)
    before = jnp.cumsum(onehot, axis=0) - onehot
    position = jnp.sum(before * onehot, axis=1)
    target = flat_ids * capacity + position
    source = (
        jnp.full((experts * capacity,), slot_count, jnp.int32)
        .at[target]
        .set(jnp.arange(slot_count, dtype=jnp.int32))
    )
    filled = source < slot_count
    clipped = jnp.minimum(source, slot_count - 1)
    token_of = clipped // top_k
    weight_of = jnp.where(filled, routing_weights.reshape(-1)[clipped], 0.0)
    rows_src = lax.dynamic_slice_in_dim(hidden_in, share_offset, feature_share, 1)
    cot_src = lax.dynamic_slice_in_dim(cotangent, share_offset, feature_share, 1)
    send_rows = jnp.where(filled[:, None], rows_src[token_of], jnp.zeros((), jnp.bfloat16))
    send_rows = send_rows.reshape(experts, capacity, -1)
    send_cot = (weight_of[:, None] * cot_src[token_of].astype(jnp.float32)).astype(jnp.bfloat16)
    send_cot = send_cot.reshape(experts, capacity, -1)
    part_rows, part_cot = (
        lax.all_to_all(send_rows, "sp", split_axis=0, concat_axis=1, tiled=True),
        lax.all_to_all(send_cot, "sp", split_axis=0, concat_axis=1, tiled=True),
    )
    rows_h, rows_s = (
        lax.all_gather(part_rows, "tp", axis=2, tiled=True),
        lax.all_gather(part_cot, "tp", axis=2, tiled=True),
    )
    pre_gate = jnp.einsum("erd,edf->erf", rows_h, w_gate, preferred_element_type=jnp.float32)
    pre_up = jnp.einsum("erd,edf->erf", rows_h, w_up, preferred_element_type=jnp.float32)
    sigma = jax.nn.sigmoid(pre_gate)
    silu_gate = pre_gate * sigma
    hid = (silu_gate * pre_up).astype(jnp.bfloat16)
    d_hid = jnp.einsum("erd,efd->erf", rows_s, w_down, preferred_element_type=jnp.float32)
    d_up = (d_hid * silu_gate).astype(jnp.bfloat16)
    d_pre = (d_hid * pre_up * sigma * (1.0 + pre_gate * (1.0 - sigma))).astype(jnp.bfloat16)
    grad_down = jnp.einsum("erf,erd->efd", hid, rows_s, preferred_element_type=jnp.float32).astype(
        jnp.bfloat16
    )
    grad_gate = jnp.einsum(
        "erd,erf->edf", rows_h, d_pre, preferred_element_type=jnp.float32
    ).astype(jnp.bfloat16)
    grad_up = jnp.einsum("erd,erf->edf", rows_h, d_up, preferred_element_type=jnp.float32).astype(
        jnp.bfloat16
    )
    partial_grad = jnp.einsum("erf,edf->erd", d_pre, w_gate, preferred_element_type=jnp.float32)
    partial_grad = partial_grad + jnp.einsum(
        "erf,edf->erd", d_up, w_up, preferred_element_type=jnp.float32
    )
    partial_low = partial_grad.astype(jnp.bfloat16)
    shared_rows = (
        lax.psum_scatter(partial_low, "tp", scatter_dimension=2, tiled=True)
        .astype(jnp.float32)
        .astype(jnp.bfloat16)
    )
    back = lax.all_to_all(shared_rows, "sp", split_axis=1, concat_axis=0, tiled=True)
    back_flat = back.reshape(experts * capacity, feature_share)
    per_token = back_flat[target].astype(jnp.float32).reshape(tok_rows, top_k, feature_share)
    own_cot = lax.dynamic_slice_in_dim(cotangent, share_offset, feature_share, 1).astype(
        jnp.float32
    )
    residual_grad = (own_cot + jnp.sum(per_token, axis=1)).astype(jnp.bfloat16)
    full_grad = lax.all_gather(residual_grad, "tp", axis=1, tiled=True)
    taps_f = taps.astype(jnp.float32)
    gated = c_gate.astype(jnp.float32) * x_in.astype(jnp.float32)
    earlier = from_behind(gated[tok_rows - 2 :], "sp", 1)
    padded = jnp.concatenate([earlier, gated], axis=0)
    conv = (
        taps_f[0] * padded[0:tok_rows]
        + taps_f[1] * padded[1 : tok_rows + 1]
        + taps_f[2] * padded[2 : tok_rows + 2]
    )
    b_f = b_gate.astype(jnp.float32)
    y_short = (b_f * conv).astype(jnp.bfloat16)
    d_y = jnp.dot(full_grad, w_out, preferred_element_type=jnp.float32)
    grad_b = (d_y * conv).astype(jnp.bfloat16)
    d_conv = b_f * d_y
    following = from_behind(d_conv[0:2], "sp", -1)
    later = jnp.concatenate([d_conv, following], axis=0)
    d_v = (
        taps_f[2] * later[0:tok_rows]
        + taps_f[1] * later[1 : tok_rows + 1]
        + taps_f[0] * later[2 : tok_rows + 2]
    )
    grad_c = (d_v * x_in.astype(jnp.float32)).astype(jnp.bfloat16)
    grad_x = (d_v * c_gate.astype(jnp.float32)).astype(jnp.bfloat16)
    out_proj_grad = lax.psum_scatter(
        jnp.einsum("td,tc->dc", full_grad, y_short, preferred_element_type=jnp.float32),
        "sp",
        scatter_dimension=0,
        tiled=True,
    )
    return (grad_gate, grad_up, grad_down, out_proj_grad, residual_grad, grad_b, grad_c, grad_x)


def solution(mesh):
    return jax.shard_map(
        per_device,
        mesh=mesh,
        in_specs=(
            P("sp", None),
            P("sp", None),
            P("sp", None),
            P("sp", None),
            P("sp", None, "tp"),
            P("sp", None, "tp"),
            P("sp", "tp", None),
            P("sp", "tp"),
            P("sp", "tp"),
            P("sp", "tp"),
            P(None, "tp"),
            P(None, "tp"),
        ),
        out_specs=(
            P("sp", None, "tp"),
            P("sp", None, "tp"),
            P("sp", "tp", None),
            P("sp", "tp"),
            P("sp", "tp"),
            P("sp", "tp"),
            P("sp", "tp"),
            P("sp", "tp"),
        ),
        check_vma=False,
    )
```

profile of v0, /device:TPU:15, one launch (start us, length us, event | category | flops | bytes accessed | tf_op | source)
XLA Modules:
  0.0 287.0 jit_solution(8759638803570472328)
XLA Ops:
  10.9 2.4 scatter_custom_fusion
  14.4 5.0 %gather_fusion.1 = f32[768]{0:T(1024)S(1)} fusion(f32[512]{0:T(512)S(1)} %reshape.162, s32[1024]{0:T(1024)S(1)} %get-tuple-element.22), kind=kCustom, calls=%fused_computation.1 | custom fusion | bytes 9216 | tf_op jit(solution)/shard_map/gather | solution.py:50
  20.5 2.7 gather_fusion
  23.3 22.6 %all_to_all.33 = bf16[8,96,512]{2,1,0:T(8,128)(2,1)} all-to-all(bf16[8,96,512]{2,1,0:T(8,128)(2,1)S(1)} %broadcast_select_fusion), channel_id=1, replica_groups=mesh['sp'=8,'tp'=4] {'sp'}, dimensions={0} | all-to-all | bytes 1572864 | tf_op jit(solution)/shard_map/all_to_all | solution.py:58
  47.0 2.7 gather_fusion.2
  50.0 23.1 %all_to_all.34 = bf16[8,96,512]{2,1,0:T(8,128)(2,1)} all-to-all(bf16[8,96,512]{2,1,0:T(8,128)(2,1)S(1)} %fusion.31), channel_id=1, replica_groups=mesh['sp'=8,'tp'=4] {'sp'}, dimensions={0} | all-to-all | bytes 1572864 | tf_op jit(solution)/shard_map/all_to_all | solution.py:59
  73.4 2.9 all-gather.4.cloned.1.call-done
  76.2 3.9 %fusion.8 = f32[768,256]{1,0:T(8,128)} fusion(bf16[1,768,2048]{2,1,0:T(8,128)(2,1)} %all-gather.4.cloned.1.call-done, bf16[1,2048,256]{2,1,0:T(8,128)(2,1)S(1)} %copy-done), kind=kOutput, calls=%fused_computation.14 | convolution fusion | flops 805306368 | bytes 4980736 | tf_op jit(solution)/shard_map/erd,edf->erf/dot_general | solution.py:65
  80.1 1.9 fusion.10
  82.0 24.3 %all-gather.6.cloned.1.call-done = bf16[1,768,2048]{2,1,0:T(8,128)(2,1)} async-done(((bf16[1,768,512]{2,1,0:T(8,128)(2,1)}), bf16[1,768,2048]{2,1,0:T(8,128)(2,1)}) %all-gather.6.cloned.1.call-update) | async-done | bytes 3145744 | tf_op jit(solution)/shard_map/all_gather | solution.py:63
  106.3 3.5 %multiply_convert_fusion.1 = (bf16[768,256]{1,0:T(8,128)(2,1)S(1)}, bf16[768,256]{1,0:T(8,128)(2,1)S(1)}) fusion(f32[768,256]{1,0:T(8,128)} %fusion.8, f32[768,256]{1,0:T(8,128)} %fusion.10, bf16[1,256,2048]{2,1,0:T(8,128)(2,1)S(1)} %copy-done.14, bf16[1,768,2048]{2,1,0:T(8,128)(2,1)} %all-gather.6.cloned.1.call-done), kind=kOutput, calls=%fused_computation.35 | convolution fusion | flops 807862272 | bytes 6553600 | tf_op jit(solution)/shard_map/erd,efd->erf/dot_general | solution.py:70
  110.9 2.7 fusion.12
  113.6 37.3 %reduce-scatter.3.cloned.1.call-done = bf16[1,768,512]{2,1,0:T(8,128)(2,1)} async-done(((bf16[1,768,2048]{2,1,0:T(8,128)(2,1)}), bf16[1,768,512]{2,1,0:T(8,128)(2,1)}) %reduce-scatter.3.cloned.1.call-update) | async-done | bytes 786448 | tf_op jit(solution)/shard_map/reduce_scatter | solution.py:88
  151.0 2.3 copy.38
  153.8 5.6 %reduce.2 = bf16[768,512]{1,0:T(8,128)(2,1)S(1)} reduce(bf16[768,1,512]{2,1,0:T(2,128)(2,1)S(1)} %bitcast.84, bf16[]{:T(256)} %broadcast.111), dimensions={1}, to_apply=%bitcast.82.reduce_sub_computation | reduce | bytes 1572866
  159.5 1.5 reshape.216
  160.9 5.5 %all-to-all-start.2 = ((bf16[8,2,24576]{2,1,0:T(2,128)(2,1)}), bf16[8,2,24576]{2,1,0:T(2,128)(2,1)S(1)}, u32[]{:S(2)}, u32[]{:S(2)}) async-start(bf16[8,2,24576]{2,1,0:T(2,128)(2,1)} %reshape.216), calls=%async_computation.3 | async-start | bytes 1572864 | tf_op jit(solution)/shard_map/all_to_all | solution.py:92
  166.4 17.6 %all-to-all-done.2 = bf16[8,2,24576]{2,1,0:T(2,128)(2,1)S(1)} async-done(((bf16[8,2,24576]{2,1,0:T(2,128)(2,1)}), bf16[8,2,24576]{2,1,0:T(2,128)(2,1)S(1)}, u32[]{:S(2)}, u32[]{:S(2)}) %all-to-all-start.2) | async-done | bytes 786464 | tf_op jit(solution)/shard_map/all_to_all | solution.py:92
  185.0 2.0 gather_fusion.3
  187.7 1.2 reduce_sum.22
  188.9 1.7 add_convert_fusion.1
  190.8 2.8 collective-permute-start
  193.6 1.5 collective-permute-done
  195.1 13.5 %all-gather.8.cloned.1.call-done = bf16[256,2048]{1,0:T(8,128)(2,1)} async-done(((bf16[256,512]{1,0:T(8,128)(2,1)}), bf16[256,2048]{1,0:T(8,128)(2,1)}) %all-gather.8.cloned.1.call-update) | async-done | bytes 1048592 | tf_op jit(solution)/shard_map/all_gather | solution.py:99
  208.6 2.7 multiply_convert_fusion.4
  211.3 1.8 fusion.53
  213.3 4.1 %fusion.28 = bf16[1,2048,256]{2,1,0:T(8,128)(2,1)} fusion(bf16[768,256]{1,0:T(8,128)(2,1)S(1)} %copy-done.2, bf16[1,768,2048]{2,1,0:T(8,128)(2,1)} %all-gather.4.cloned.1.call-done), kind=kOutput, calls=%fused_computation.24 | convolution fusion | flops 805830656 | bytes 4587520 | tf_op jit(solution)/shard_map/erd,erf->edf/dot_general | solution.py:76
  217.3 2.0 fusion.22
  219.4 2.2 collective-permute-start.1
  221.6 2.0 fusion.25
  223.6 1.5 collective-permute-done.1
  226.5 53.9 %reduce-scatter.5.cloned.1.call-done = f32[256,256]{1,0:T(8,128)} async-done(((f32[2048,256]{1,0:T(8,128)}), f32[256,256]{1,0:T(8,128)}) %reduce-scatter.5.cloned.1.call-update) | async-done | bytes 262160 | tf_op jit(solution)/shard_map/reduce_scatter | solution.py:123
  (81 shorter events, 12.3 us)
Async XLA Ops:
  7.2 69.1 %copy-start = (bf16[1,2048,256]{2,1,0:T(8,128)(2,1)S(1)}, bf16[1,2048,256]{2,1,0:T(8,128)(2,1)}, u32[]{:S(2)}) copy-start(bf16[1,2048,256]{2,1,0:T(8,128)(2,1)} %param.16) | copy-start | bytes 3145732
  7.2 69.1 %all-gather.4.cloned.1.call-start = ((), (), s32[]{:S(2)}) async-start(), calls=%async_computation.5 | async-start | bytes 3932160 | tf_op jit(solution)/shard_map/all_gather | solution.py:62
  46.0 60.3 %all-gather.6.cloned.1.call-start = ((), (), s32[]{:S(2)}) async-start(), calls=%async_computation.6 | async-start | bytes 3932160 | tf_op jit(solution)/shard_map/all_gather | solution.py:63
  73.1 7.0 %copy-start.4 = (bf16[1,2048,256]{2,1,0:T(8,128)(2,1)S(1)}, bf16[1,2048,256]{2,1,0:T(8,128)(2,1)}, u32[]{:S(2)}) copy-start(bf16[1,2048,256]{2,1,0:T(8,128)(2,1)} %param.17) | copy-start | bytes 3145732
  73.1 77.8 %reduce-scatter.3.cloned.1.call-start = ((), (), s32[]{:S(2)}) async-start(), calls=%async_computation.7 | async-start | bytes 3932160 | tf_op jit(solution)/shard_map/reduce_scatter | solution.py:88
  76.2 3.9 %copy-start.11 = (bf16[1,768,2048]{2,1,0:T(8,128)(2,1)S(1)}, bf16[1,768,2048]{2,1,0:T(8,128)(2,1)}, u32[]{:S(2)}) copy-start(bf16[1,768,2048]{2,1,0:T(8,128)(2,1)} %all-gather.4.cloned.1.call-done) | copy-start | bytes 9437188
  80.1 26.2 %copy-start.14 = (bf16[1,256,2048]{2,1,0:T(8,128)(2,1)S(1)}, bf16[1,256,2048]{2,1,0:T(8,128)(2,1)}, u32[]{:S(2)}) copy-start(bf16[1,256,2048]{2,1,0:T(8,128)(2,1)} %param.18) | copy-start | bytes 3145732
  109.8 1.0 copy-start.1
  109.8 1.0 copy-start.7
  160.9 23.0 %all-to-all-start.2 = ((bf16[8,2,24576]{2,1,0:T(2,128)(2,1)}), bf16[8,2,24576]{2,1,0:T(2,128)(2,1)S(1)}, u32[]{:S(2)}, u32[]{:S(2)}) async-start(bf16[8,2,24576]{2,1,0:T(2,128)(2,1)} %reshape.216), calls=%async_computation.3 | async-start | bytes 1572864 | tf_op jit(solution)/shard_map/all_to_all | solution.py:92
  166.4 42.2 %all-gather.8.cloned.1.call-start = ((), (), s32[]{:S(2)}) async-start(), calls=%async_computation.8 | async-start | bytes 1310720 | tf_op jit(solution)/shard_map/all_gather | solution.py:99
  186.9 3.8 %copy-start.5 = (bf16[256,256]{1,0:T(8,128)(2,1)S(1)}, bf16[256,256]{1,0:T(8,128)(2,1)}, u32[]{:S(2)}) copy-start(bf16[256,256]{1,0:T(8,128)(2,1)} %param.20) | copy-start | bytes 393220
  187.0 3.8 %copy-start.6 = (bf16[256,256]{1,0:T(8,128)(2,1)S(1)}, bf16[256,256]{1,0:T(8,128)(2,1)}, u32[]{:S(2)}) copy-start(bf16[256,256]{1,0:T(8,128)(2,1)} %param.21) | copy-start | bytes 393220
  187.0 6.6 %copy-start.10 = (bf16[3,256]{1,0:T(4,128)(2,1)S(1)}, bf16[3,256]{1,0:T(4,128)(2,1)}, u32[]{:S(2)}) copy-start(bf16[3,256]{1,0:T(4,128)(2,1)} %param.22) | copy-start | bytes 4612
  187.0 21.6 %copy-start.9 = (bf16[256,256]{1,0:T(8,128)(2,1)S(1)}, bf16[256,256]{1,0:T(8,128)(2,1)}, u32[]{:S(2)}) copy-start(bf16[256,256]{1,0:T(8,128)(2,1)} %param.19) | copy-start | bytes 393220
  190.7 89.8 %reduce-scatter.5.cloned.1.call-start = ((), (), s32[]{:S(2)}) async-start(), calls=%async_computation.9 | async-start | bytes 2359296 | tf_op jit(solution)/shard_map/reduce_scatter | solution.py:123
  190.8 4.3 %collective-permute-start = (f32[2,256]{1,0:T(2,128)S(1)}, f32[2,256]{1,0:T(2,128)S(1)}, u32[]{:S(2)}, u32[]{:S(2)}) collective-permute-start(f32[2,256]{1,0:T(2,128)S(1)} %slice.57), channel_id=1, source_target_pairs={{0,4},{4,8},{8,12},{12,16},{16,20},{20,24},{24,28},{1,5},{5,9},{9,... | collective-permute-start | bytes 6152 | tf_op jit(solution)/shard_map/ppermute | solution.py:10
  208.6 2.7 copy-start.3
  211.3 1.9 copy-start.2
  213.2 4.1 %copy-start.13 = (bf16[1,768,2048]{2,1,0:T(8,128)(2,1)S(1)}, bf16[1,768,2048]{2,1,0:T(8,128)(2,1)}, u32[]{:S(2)}) copy-start(bf16[1,768,2048]{2,1,0:T(8,128)(2,1)} %all-gather.6.cloned.1.call-done) | copy-start | bytes 9437188
  213.2 4.1 %copy-start.15 = (f32[768,256]{1,0:T(8,128)S(1)}, f32[768,256]{1,0:T(8,128)}, u32[]{:S(2)}) copy-start(f32[768,256]{1,0:T(8,128)} %fusion.8) | copy-start | bytes 2359300
  213.2 4.1 %copy-start.16 = (f32[768,256]{1,0:T(8,128)S(1)}, f32[768,256]{1,0:T(8,128)}, u32[]{:S(2)}) copy-start(f32[768,256]{1,0:T(8,128)} %fusion.10) | copy-start | bytes 2359300
  217.3 4.2 %copy-start.8 = (bf16[768,256]{1,0:T(8,128)(2,1)S(1)}, bf16[768,256]{1,0:T(8,128)(2,1)}, u32[]{:S(2)}) copy-start(bf16[768,256]{1,0:T(8,128)(2,1)} %copy-done.7) | copy-start | bytes 1179652
  217.3 4.2 %copy-start.12 = (bf16[1,768,2048]{2,1,0:T(8,128)(2,1)S(1)}, bf16[1,768,2048]{2,1,0:T(8,128)(2,1)}, u32[]{:S(2)}) copy-start(bf16[1,768,2048]{2,1,0:T(8,128)(2,1)} %all-gather.4.cloned.1.call-done) | copy-start | bytes 9437188
  219.4 5.7 %collective-permute-start.1 = (f32[2,256]{1,0:T(2,128)S(1)}, f32[2,256]{1,0:T(2,128)S(1)}, u32[]{:S(2)}, u32[]{:S(2)}) collective-permute-start(f32[2,256]{1,0:T(2,128)S(1)} %slice.62), channel_id=1, source_target_pairs={{4,0},{8,4},{12,8},{16,12},{20,16},{24,20},{28,24},{5,1},{9,5},{13... | collective-permute-start | bytes 6152 | tf_op jit(solution)/shard_map/ppermute | solution.py:10
Sparse Core Ops, SparseCore 0:
  46.1 30.0 all-gather.3
  77.8 28.4 all-gather.5
  113.8 37.1 reduce-scatter.2
  190.8 17.7 all-gather.7
  213.3 67.0 reduce-scatter.4
where the time goes:
time: 291 us; the launch traced here: 287 us
  waiting for transfers between devices  152 us (52%)
  blocking collectives  45.7 us (16%)
  matrix products  25.7 us (9%)
  local copies, waits for them, and re-layouts  25.5 us (9%)
  between operations  14.2 us (5%)
  other arithmetic  12.6 us (4%)
  starting transfers between devices  10.8 us (4%)
    reduce_scatter x1, waiting for transfers between devices, per_device(): lax.psum_scatter(jnp.einsum('td,tc->dc', full_grad, y_short, preferred_el...  53.9 us
    reduce_scatter x1, waiting for transfers between devices, per_device(): lax.psum_scatter(partial_low, 'tp', scatter_dimension=2, tiled=True)  37.3 us
    all_gather x1, waiting for transfers between devices, per_device(): lax.all_gather(part_cot, 'tp', axis=2, tiled=True)  24.3 us
    all_to_all x1, blocking collectives, per_device(): lax.all_to_all(send_cot, 'sp', split_axis=0, concat_axis=1, tiled=True)  23.1 us
    all_to_all x1, blocking collectives, per_device(): lax.all_to_all(send_rows, 'sp', split_axis=0, concat_axis=1, tiled=True)  22.6 us
    all_to_all x1, waiting for transfers between devices, per_device(): lax.all_to_all(shared_rows, 'sp', split_axis=1, concat_axis=0, tiled=True)  17.6 us
    all_gather x1, waiting for transfers between devices, per_device(): full_grad = lax.all_gather(residual_grad, 'tp', axis=1, tiled=True)  13.5 us
  transfers between devices with their start and end apart: 8, of which 8 were waited for; matrix products, arithmetic and copies ran while one was open for 7% of the time, Pallas kernels for 0%

commit v1 on v0

v1 whole, which is shorter than its diff:
```python
import functools

import jax
import jax.numpy as jnp
from jax import lax
from jax.experimental import pallas as pl
from jax.experimental.pallas import tpu as pltpu
from jax.sharding import PartitionSpec as P

MESH = pl.DeviceIdType.MESH
BF16, F32 = jnp.bfloat16, jnp.float32
VMEM = pl.BlockSpec(memory_space=pltpu.VMEM)


def coordinates(sp_size, tp_size):
    me, mine = lax.axis_index("sp"), lax.axis_index("tp")
    near = mine + 1 - 2 * (mine % 2)
    far = (mine + tp_size // 2) % tp_size
    return me, mine, near, far


def greet(sp_size, me, tp_partners):
    barrier = pltpu.get_barrier_semaphore()

    def one(i, carry):
        pl.semaphore_signal(
            barrier, inc=1, device_id={"sp": (me + 1 + i) % sp_size}, device_id_type=MESH
        )
        return carry

    lax.fori_loop(0, sp_size - 1, one, 0)
    for partner in tp_partners:
        pl.semaphore_signal(barrier, inc=1, device_id={"tp": partner}, device_id_type=MESH)
    pl.semaphore_wait(barrier, sp_size - 1 + len(tp_partners))


def remote(src, dst, send_sem, recv_sem, to):
    return pltpu.make_async_remote_copy(
        src_ref=src,
        dst_ref=dst,
        send_sem=send_sem,
        recv_sem=recv_sem,
        device_id=to,
        device_id_type=MESH,
    )


def each(count, body):
    def step(i, carry):
        body(i)
        return carry

    lax.fori_loop(0, count, step, 0)


def dispatch_kernel(sp_size, tp_size, send, own, tail, rows, earlier, sems, own_sem, tail_sems):
    me, mine, near, far = coordinates(sp_size, tp_size)
    share = send.shape[3]

    def columns(owner):
        return pl.ds(pl.multiple_of(owner * share, 128), share)

    keep = pltpu.make_async_copy(own, rows.at[:, me], own_sem)
    keep.start()
    greet(sp_size, me, (near, far))
    halo = remote(tail, earlier, tail_sems.at[0], tail_sems.at[1], {"sp": (me + 1) % sp_size})
    halo.start()

    def out(i):
        to = (me + 1 + i) % sp_size
        return remote(
            send.at[:, to],
            rows.at[:, me, :, columns(mine)],
            sems.at[0, i],
            sems.at[1, i],
            {"sp": to},
        )

    def onward(i, owner, lane, partner):
        block = rows.at[:, (me + sp_size - 1 - i) % sp_size, :, columns(owner)]
        return remote(block, block, sems.at[2 * lane, i], sems.at[2 * lane + 1, i], {"tp": partner})

    each(sp_size - 1, lambda i: out(i).start())

    def cross(i):
        onward(i, mine, 1, far).wait_recv()
        onward(i, far, 3, near).start()

    def arrive(i):
        out(i).wait_recv()
        onward(i, mine, 1, far).start()
        onward(i, mine, 2, near).start()
        pl.when(i > 0)(lambda: cross(i - 1))

    each(sp_size - 1, arrive)
    cross(sp_size - 2)

    def finish(i):
        out(i).wait_send()
        onward(i, mine, 1, far).wait_send()
        onward(i, mine, 2, near).wait()
        onward(i, far, 3, near).wait()

    each(sp_size - 1, finish)
    halo.wait()
    keep.wait()


def combine_kernel(
    sp_size,
    tp_size,
    d_pre,
    d_up,
    w_gate,
    w_up,
    place,
    cotangent,
    residual,
    full,
    near_out,
    near_in,
    kept,
    far_out,
    far_in,
    back_out,
    back,
    total,
    sems,
    all_sems,
):
    me, mine, near, far = coordinates(sp_size, tp_size)
    share = residual.shape[1]
    near_far = (near + tp_size // 2) % tp_size
    greet(sp_size, me, (near, far))

    def rows_of(owner):
        return pl.ds(pl.multiple_of(owner * share, 128), share)

    def product(which, owner):
        dims = (((1,), (1,)), ((), ()))
        return lax.dot_general(
            d_pre[which], w_gate[rows_of(owner), :], dims, preferred_element_type=F32
        ) + lax.dot_general(d_up[which], w_up[rows_of(owner), :], dims, preferred_element_type=F32)

    def across(i):
        return remote(near_out.at[i], near_in.at[i], sems.at[0, i], sems.at[1, i], {"tp": near})

    def over(i):
        return remote(far_out.at[i], far_in.at[i], sems.at[2, i], sems.at[3, i], {"tp": far})

    def home(i):
        return remote(
            back_out.at[i],
            back.at[me],
            sems.at[4, i],
            sems.at[5, i],
            {"sp": (me + 1 + i) % sp_size},
        )

    def second(i):
        across(i).wait_recv()
        far_out[i] = (kept[i, 1] + near_in[i, 1].astype(F32)).astype(BF16)
        over(i).start()

    def first(i):
        which = (me + 1 + i) % sp_size
        near_out[i, 0] = product(which, near).astype(BF16)
        near_out[i, 1] = product(which, near_far).astype(BF16)
        across(i).start()
        kept[i, 0] = product(which, mine)
        kept[i, 1] = product(which, far)
        pl.when(i > 0)(lambda: second(i - 1))

    each(sp_size, first)
    second(sp_size - 1)

    def summed(i):
        over(i).wait_recv()
        return (kept[i, 0] + near_in[i, 0].astype(F32) + far_in[i].astype(F32)).astype(BF16)

    def third(i):
        back_out[i] = summed(i)
        home(i).start()

    each(sp_size - 1, third)
    total[...] = cotangent[...].astype(F32) + jnp.dot(
        place[me], summed(sp_size - 1), preferred_element_type=F32
    )

    def collect(i):
        home(i).wait_recv()
        expert = (me + sp_size - 1 - i) % sp_size
        total[...] += jnp.dot(place[expert], back[expert], preferred_element_type=F32)

    each(sp_size - 1, collect)
    result = total[...].astype(BF16)
    residual[...] = result
    full[:, rows_of(mine)] = result

    def gathered(owner, lane, partner):
        block = full.at[:, rows_of(owner)]
        return remote(block, block, all_sems.at[2 * lane], all_sems.at[2 * lane + 1], {"tp": partner})

    to_far, to_near = gathered(mine, 0, far), gathered(mine, 1, near)
    to_far.start()
    to_near.start()
    to_far.wait_recv()
    forward = gathered(far, 2, near)
    forward.start()

    def finish(i):
        across(i).wait_send()
        over(i).wait_send()

    each(sp_size, finish)
    each(sp_size - 1, lambda i: home(i).wait_send())
    to_far.wait_send()
    to_near.wait()
    forward.wait()


def reduce_kernel(sp_size, part, head, out, following, land, sems, head_sems):
    me = lax.axis_index("sp")
    greet(sp_size, me, ())
    halo = remote(
        head, following, head_sems.at[0], head_sems.at[1], {"sp": (me + sp_size - 1) % sp_size}
    )
    halo.start()

    def piece(i):
        to = (me + 1 + i) % sp_size
        return remote(part.at[to], land.at[i], sems.at[0, i], sems.at[1, i], {"sp": to})

    each(sp_size - 1, lambda i: piece(i).start())
    out[...] = part[me].astype(F32)

    def add(i):
        piece(i).wait_recv()
        out[...] += land[i].astype(F32)

    each(sp_size - 1, add)
    each(sp_size - 1, lambda i: piece(i).wait_send())
    halo.wait()


def communicate(kernel, number, inputs, outputs, scratch):
    return pl.pallas_call(
        kernel,
        out_shape=[jax.ShapeDtypeStruct(shape, kind) for shape, kind in outputs],
        in_specs=[VMEM] * len(inputs),
        out_specs=[VMEM] * len(outputs),
        scratch_shapes=scratch,
        compiler_params=pltpu.CompilerParams(collective_id=number, has_side_effects=True),
    )(*inputs)


def per_device(
    hidden_in,
    cotangent,
    routes,
    routing_weights,
    w_gate,
    w_up,
    w_down,
    b_gate,
    c_gate,
    x_in,
    taps,
    w_out,
):
    tok_rows, model_width = hidden_in.shape
    top_k = routes.shape[1]
    sp_size = lax.axis_size("sp")
    tp_size = lax.axis_size("tp")
    experts = w_gate.shape[0] * sp_size
    capacity = 3 * tok_rows * top_k // (2 * experts)
    share = model_width // tp_size
    channels = x_in.shape[1]
    offset = lax.axis_index("tp") * share
    me = lax.axis_index("sp")
    w_gate, w_up, w_down = w_gate[0], w_up[0], w_down[0]

    expert_ids = jnp.arange(experts, dtype=jnp.int32)
    hit = routes[:, :, None] == expert_ids[None, None, :]
    member = jnp.any(hit, axis=1)
    weight = jnp.sum(jnp.where(hit, routing_weights[:, :, None], 0.0), axis=1)
    lower = jnp.tri(tok_rows, k=-1, dtype=BF16)
    position = jnp.dot(lower, member.astype(BF16), preferred_element_type=F32).astype(jnp.int32)
    position = jnp.where(member, position, -1)
    slots = jnp.arange(capacity, dtype=jnp.int32)
    taken = position.T[:, None, :] == slots[None, :, None]
    select = taken.astype(BF16)
    place = (position.T[:, :, None] == slots[None, None, :]).astype(BF16)
    slot_weight = jnp.sum(jnp.where(taken, weight.T[:, None, :], 0.0), axis=2)

    def pick(chosen, weights, rows_src, cot_src):
        rows = jnp.einsum("...t,td->...d", chosen, rows_src, preferred_element_type=F32)
        cot = jnp.einsum("...t,td->...d", chosen, cot_src, preferred_element_type=F32)
        return jnp.stack([rows.astype(BF16), (weights[..., None] * cot).astype(BF16)])

    rows_src = lax.dynamic_slice_in_dim(hidden_in, offset, share, 1)
    cot_src = lax.dynamic_slice_in_dim(cotangent, offset, share, 1)
    send = pick(select, slot_weight, rows_src, cot_src)
    own = pick(select[me], slot_weight[me], hidden_in, cotangent)

    c_f, x_f, b_f = c_gate.astype(F32), x_in.astype(F32), b_gate.astype(F32)
    gated = c_f * x_f
    rows, earlier = communicate(
        functools.partial(dispatch_kernel, sp_size, tp_size),
        0,
        (send, own, gated[tok_rows - 8 :]),
        [((2, sp_size, capacity, model_width), BF16), ((8, channels), F32)],
        [
            pltpu.SemaphoreType.DMA((8, sp_size - 1)),
            pltpu.SemaphoreType.DMA,
            pltpu.SemaphoreType.DMA((2,)),
        ],
    )
    rows_h = rows[0].reshape(sp_size * capacity, model_width)
    rows_s = rows[1].reshape(sp_size * capacity, model_width)

    pre_gate = jnp.dot(rows_h, w_gate, preferred_element_type=F32)
    pre_up = jnp.dot(rows_h, w_up, preferred_element_type=F32)
    sigma = jax.nn.sigmoid(pre_gate)
    silu_gate = pre_gate * sigma
    hid = (silu_gate * pre_up).astype(BF16)
    d_hid = jnp.einsum("rd,fd->rf", rows_s, w_down, preferred_element_type=F32)
    d_up = (d_hid * silu_gate).astype(BF16)
    d_pre = (d_hid * pre_up * sigma * (1.0 + pre_gate * (1.0 - sigma))).astype(BF16)
    grad_down = jnp.einsum("rf,rd->fd", hid, rows_s, preferred_element_type=F32).astype(BF16)
    grad_gate = jnp.einsum("rd,rf->df", rows_h, d_pre, preferred_element_type=F32).astype(BF16)
    grad_up = jnp.einsum("rd,rf->df", rows_h, d_up, preferred_element_type=F32).astype(BF16)

    residual_grad, full_grad = communicate(
        functools.partial(combine_kernel, sp_size, tp_size),
        1,
        (
            d_pre.reshape(sp_size, capacity, -1),
            d_up.reshape(sp_size, capacity, -1),
            w_gate,
            w_up,
            place,
            cot_src,
        ),
        [((tok_rows, share), BF16), ((tok_rows, model_width), BF16)],
        [
            pltpu.VMEM((sp_size, 2, capacity, share), BF16),
            pltpu.VMEM((sp_size, 2, capacity, share), BF16),
            pltpu.VMEM((sp_size, 2, capacity, share), F32),
            pltpu.VMEM((sp_size, capacity, share), BF16),
            pltpu.VMEM((sp_size, capacity, share), BF16),
            pltpu.VMEM((sp_size, capacity, share), BF16),
            pltpu.VMEM((sp_size, capacity, share), BF16),
            pltpu.VMEM((tok_rows, share), F32),
            pltpu.SemaphoreType.DMA((6, sp_size)),
            pltpu.SemaphoreType.DMA((6,)),
        ],
    )

    taps_f = taps.astype(F32)
    earlier = jnp.where(me == 0, 0.0, earlier[6:])
    padded = jnp.concatenate([earlier, gated], axis=0)
    conv = (
        taps_f[0] * padded[0:tok_rows]
        + taps_f[1] * padded[1 : tok_rows + 1]
        + taps_f[2] * padded[2 : tok_rows + 2]
    )
    y_short = (b_f * conv).astype(BF16)
    d_y = jnp.dot(full_grad, w_out, preferred_element_type=F32)
    grad_b = (d_y * conv).astype(BF16)
    d_conv = b_f * d_y
    part = jnp.einsum("td,tc->dc", full_grad, y_short, preferred_element_type=F32).astype(BF16)
    block = model_width // sp_size
    out_proj_grad, following = communicate(
        functools.partial(reduce_kernel, sp_size),
        2,
        (part.reshape(sp_size, block, channels), d_conv[:8]),
        [((block, channels), F32), ((8, channels), F32)],
        [
            pltpu.VMEM((sp_size - 1, block, channels), BF16),
            pltpu.SemaphoreType.DMA((2, sp_size - 1)),
            pltpu.SemaphoreType.DMA((2,)),
        ],
    )
    following = jnp.where(me == sp_size - 1, 0.0, following[:2])
    later = jnp.concatenate([d_conv, following], axis=0)
    d_v = (
        taps_f[2] * later[0:tok_rows]
        + taps_f[1] * later[1 : tok_rows + 1]
        + taps_f[0] * later[2 : tok_rows + 2]
    )
    grad_c = (d_v * x_f).astype(BF16)
    grad_x = (d_v * c_f).astype(BF16)
    grads = (grad_gate[None], grad_up[None], grad_down[None])
    return grads + (out_proj_grad, residual_grad, grad_b, grad_c, grad_x)


def solution(mesh):
    return jax.shard_map(
        per_device,
        mesh=mesh,
        in_specs=(
            P("sp", None),
            P("sp", None),
            P("sp", None),
            P("sp", None),
            P("sp", None, "tp"),
            P("sp", None, "tp"),
            P("sp", "tp", None),
            P("sp", "tp"),
            P("sp", "tp"),
            P("sp", "tp"),
            P(None, "tp"),
            P(None, "tp"),
        ),
        out_specs=(
            P("sp", None, "tp"),
            P("sp", None, "tp"),
            P("sp", "tp", None),
            P("sp", "tp"),
            P("sp", "tp"),
            P("sp", "tp"),
            P("sp", "tp"),
            P("sp", "tp"),
        ),
        check_vma=False,
    )
```

time: 291 us -> 172 us (0.59); the launches traced: 287 us -> 172 us
  waiting for transfers between devices: 152 us -> 0 us
  Pallas kernels: 0 us -> 134 us
  blocking collectives: 45.7 us -> 0 us
  local copies, waits for them, and re-layouts: 25.5 us -> 9.24 us
  between operations: 14.2 us -> 0.91 us
  starting transfers between devices: 10.8 us -> 0 us
  matrix products: 25.7 us -> 19.6 us
  other arithmetic: 12.6 us -> 8.17 us
    pallas_call x0 -> x3, Pallas kernels: none -> 134 us  [communicate(): pl.pallas_call(kernel, out_shape=[jax.ShapeDtypeStruct(shape, kind) for s...]
    reduce_scatter x2 -> x0, waiting for transfers between devices: 91.2 us -> none  [the longest x1 53.9 us: per_device(): lax.psum_scatter(jnp.einsum('td,tc->dc', full_grad, y_short, preferred_el...]
    all_to_all x2 -> x0, blocking collectives: 45.7 us -> none  [the longest x1 23.1 us: per_device(): lax.all_to_all(send_cot, 'sp', split_axis=0, concat_axis=1, tiled=True)]
    all_gather x3 -> x0, waiting for transfers between devices: 40.7 us -> none  [the longest x1 24.3 us: per_device(): lax.all_gather(part_cot, 'tp', axis=2, tiled=True)]
    all_to_all x1 -> x0, waiting for transfers between devices: 17.6 us -> none  [per_device(): lax.all_to_all(shared_rows, 'sp', split_axis=1, concat_axis=0, tiled=True)]
    gather x4 -> x0, local copies, waits for them, and re-layouts: 12.3 us -> none  [the longest x1 5.01 us: per_device(): weight_of = jnp.where(filled, routing_weights.reshape(-1)[clipped], 0.0)]
    dot_general x10 -> x13, matrix products: 25.7 us -> 19.6 us  [the longest x1 4.52 us: per_device(): jnp.einsum('rf,rd->fd', hid, rows_s, preferred_element_type=F32)]
    unnamed x1 -> x0, other arithmetic: 5.64 us -> none
  transfers between devices with their start and end apart: 8 -> 0, of which waited for: 8 -> 0; matrix products, arithmetic and copies ran while one was open for 7% -> 0% of each run, Pallas kernels for 0% -> 0%
where the time goes in v1:
time: 172 us
  Pallas kernels  134 us (78%)
  matrix products  19.6 us (11%)
  local copies, waits for them, and re-layouts  9.24 us (5%)
  other arithmetic  8.17 us (5%)
    pallas_call x3, Pallas kernels, communicate(): pl.pallas_call(kernel, out_shape=[jax.ShapeDtypeStruct(shape, kind) for s...  134 us
    dot_general x1, matrix products, per_device(): jnp.einsum('rf,rd->fd', hid, rows_s, preferred_element_type=F32)  4.52 us
    slice x1, local copies, waits for them, and re-layouts, per_device(): rows_s = rows[1].reshape(sp_size * capacity, model_width)  3.5 us
    unnamed x44, local copies, waits for them, and re-layouts  3.48 us

profile of v1, /device:TPU:15, one launch (start us, length us, event | category | flops | bytes accessed | tf_op | source)
XLA Modules:
  0.0 171.7 jit_solution(843067902593914537)
XLA Ops:
  0.7 0.8 fusion.38
  1.7 0.7 select_reduce_fusion.1
  2.8 1.5 fusion.5
  4.3 0.3 fusion.4
  4.6 1.0 pad_maximum_fusion.1.own
  5.6 1.0 constant_dynamic-slice_fusion.1.cotangent
  6.6 0.4 fusion.7
  7.0 0.4 fusion.6
  7.4 1.3 pad_maximum_fusion.send
  8.7 0.6 slice.55.tail
  9.4 53.0 %shard_map.179 = (bf16[2,8,96,2048]{3,2,1,0:T(8,128)(2,1)}, f32[8,256]{1,0:T(8,128)}) custom-call(bf16[2,8,96,512]{3,2,1,0:T(8,128)(2,1)} %pad_maximum_fusion.send, bf16[2,96,2048]{2,1,0:T(8,128)(2,1)} %pad_maximum_fusion.1.own, f32[8,256]{1,0:T(8,128)} %slice.55.tail), custom_call_target="tpu_custom_call" | custom-call | tf_op jit(solution)/shard_map/pallas_call | solution.py:247
  62.4 3.5 %fusion.50 = (bf16[1,8,96,2048]{3,2,1,0:T(8,128)(2,1)S(1)}, bf16[1,8,96,2048]{3,2,1,0:T(8,128)(2,1)S(1)}) fusion(bf16[2,8,96,2048]{3,2,1,0:T(8,128)(2,1)} %get-tuple-element.14), kind=kLoop, calls=%fused_computation.84 | loop fusion | bytes 12582912 | tf_op jit(solution)/shard_map/slice | solution.py:320
  65.9 1.0 fusion.43
  66.9 1.0 copy-done.6
  67.9 1.0 fusion.45
  68.9 1.0 copy-done.18
  69.9 2.1 %multiply_convert_fusion.2 = (bf16[768,256]{1,0:T(8,128)(2,1)}, bf16[768,256]{1,0:T(8,128)(2,1)}) fusion(f32[768,256]{1,0:T(8,128)S(1)} %fusion.43, f32[768,256]{1,0:T(8,128)S(1)} %fusion.45, bf16[768,2048]{1,0:T(8,128)(2,1)S(1)} %bitcast.68, bf16[1,256,2048]{2,1,0:T(8,128)(2,1)S(1)} %copy-done.18), kind=kOutput, calls=%fused_computation.25 | convolution fusion | flops 807862272 | bytes 6553600 | tf_op jit(solution)/shard_map/rd,fd->rf/dot_general | solution.py:327
  72.0 1.1 fusion.11.place
  73.2 51.5 %shard_map.180 = (bf16[256,512]{1,0:T(8,128)(2,1)}, bf16[256,2048]{1,0:T(8,128)(2,1)}) custom-call(bf16[8,96,256]{2,1,0:T(8,128)(2,1)} %bitcast.72, bf16[8,96,256]{2,1,0:T(8,128)(2,1)} %bitcast.73, bf16[2048,256]{1,0:T(8,128)(2,1)} %bitcast.70, bf16[2048,256]{1,0:T(8,128)(2,1)} %bitcast.71, bf16[8,256,96]{2,1,0:T(8,128)(2,1)} %fusion.11.place, ...), custom_call_target="tpu_custom_call" | custom-call | tf_op jit(solution)/shard_map/pallas_call | solution.py:247
  124.7 0.8 slice_select_fusion.1
  125.5 2.6 %multiply_convert_fusion.5 = (bf16[256,256]{1,0:T(8,128)(2,1)}, f32[256,256]{1,0:T(8,128)S(1)}, f32[256,256]{1,0:T(8,128)S(1)}) fusion(f32[256,256]{1,0:T(8,128)S(1)} %copy-done.13, f32[256]{0:T(256)S(1)} %bitcast.79, f32[2,256]{1,0:T(2,128)S(1)} %slice_select_fusion.1, f32[256]{0:T(256)S(1)} %bitcast.77, f32[256]{0:T(256)S(1)} %bitcast.75, ...), kind=kOutput, calls=%fused_computation.59 | convolution fusion | flops 269156352 | bytes 3150848 | tf_op jit(solution)/shard_map/dot_general | solution.py:369
  128.2 1.5 convolution_convert_fusion
  129.6 0.6 slice.61.head
  130.2 29.3 %shard_map.181 = (f32[256,256]{1,0:T(8,128)}, f32[8,256]{1,0:T(8,128)}) custom-call(bf16[8,256,256]{2,1,0:T(8,128)(2,1)} %bitcast.63, f32[8,256]{1,0:T(8,128)} %slice.61.head), custom_call_target="tpu_custom_call" | custom-call | tf_op jit(solution)/shard_map/pallas_call | solution.py:247
  159.5 0.7 slice_select_fusion
  160.2 0.8 fusion.23
  161.0 0.7 fusion.24
  161.7 4.5 %fusion.2 = bf16[1,256,2048]{2,1,0:T(8,128)(2,1)} fusion(bf16[768,2048]{1,0:T(8,128)(2,1)} %bitcast.69, f32[768,256]{1,0:T(8,128)} %copy-done.20, f32[768,256]{1,0:T(8,128)} %copy-done.19), kind=kOutput, calls=%fused_computation.6 | convolution fusion | flops 807010304 | bytes 5767168 | tf_op jit(solution)/shard_map/rf,rd->fd/dot_general | solution.py:330
  166.2 2.0 %fusion.1 = bf16[1,2048,256]{2,1,0:T(8,128)(2,1)} fusion(bf16[768,2048]{1,0:T(8,128)(2,1)S(1)} %bitcast.66, bf16[768,256]{1,0:T(8,128)(2,1)S(1)} %copy-done.11), kind=kOutput, calls=%fused_computation.5 | convolution fusion | flops 805830656 | bytes 4587520 | tf_op jit(solution)/shard_map/rd,rf->df/dot_general | solution.py:332
  168.2 2.0 %fusion = bf16[1,2048,256]{2,1,0:T(8,128)(2,1)} fusion(bf16[768,2048]{1,0:T(8,128)(2,1)S(1)} %bitcast.67, bf16[768,256]{1,0:T(8,128)(2,1)S(1)} %copy-done.10), kind=kOutput, calls=%fused_computation.4 | convolution fusion | flops 805830656 | bytes 4587520 | tf_op jit(solution)/shard_map/rd,rf->df/dot_general | solution.py:331
  170.3 0.7 copy.27
  171.0 0.7 copy.28
  (47 shorter events, 0.7 us)
Async XLA Ops:
  0.6 3.7 %copy-start = (bf16[256,2048]{1,0:T(8,128)(2,1)S(1)}, bf16[256,2048]{1,0:T(8,128)(2,1)}, u32[]{:S(2)}) copy-start(bf16[256,2048]{1,0:T(8,128)(2,1)} %param.12) | copy-start | bytes 3145732
  5.6 3.1 %copy-start.8 = (bf16[256,256]{1,0:T(8,128)(2,1)S(1)}, bf16[256,256]{1,0:T(8,128)(2,1)}, u32[]{:S(2)}) copy-start(bf16[256,256]{1,0:T(8,128)(2,1)} %param.20) | copy-start | bytes 393220
  5.6 3.1 %copy-start.9 = (bf16[256,256]{1,0:T(8,128)(2,1)S(1)}, bf16[256,256]{1,0:T(8,128)(2,1)}, u32[]{:S(2)}) copy-start(bf16[256,256]{1,0:T(8,128)(2,1)} %param.21) | copy-start | bytes 393220
  6.6 55.7 %copy-start.4 = (bf16[256,512]{1,0:T(8,128)(2,1)}, bf16[256,512]{1,0:T(8,128)(2,1)S(1)}, u32[]{:S(2)}) copy-start(bf16[256,512]{1,0:T(8,128)(2,1)S(1)} %constant_dynamic-slice_fusion.1.cotangent) | copy-start | bytes 786436
  8.7 53.6 %copy-start.12 = (f32[256,256]{1,0:T(8,128)}, f32[256,256]{1,0:T(8,128)S(1)}, u32[]{:S(2)}) copy-start(f32[256,256]{1,0:T(8,128)S(1)} %convert_multiply_fusion.3) | copy-start | bytes 786436
  62.4 3.6 %copy-start.5 = (bf16[1,2048,256]{2,1,0:T(8,128)(2,1)S(1)}, bf16[1,2048,256]{2,1,0:T(8,128)(2,1)}, u32[]{:S(2)}) copy-start(bf16[1,2048,256]{2,1,0:T(8,128)(2,1)} %param.16) | copy-start | bytes 3145732
  65.9 3.0 %copy-start.1 = (bf16[1,8,96,2048]{3,2,1,0:T(8,128)(2,1)}, bf16[1,8,96,2048]{3,2,1,0:T(8,128)(2,1)S(1)}, u32[]{:S(2)}) copy-start(bf16[1,8,96,2048]{3,2,1,0:T(8,128)(2,1)S(1)} %get-tuple-element.25) | copy-start | bytes 9437188
  65.9 3.1 %copy-start.3 = (bf16[1,8,96,2048]{3,2,1,0:T(8,128)(2,1)}, bf16[1,8,96,2048]{3,2,1,0:T(8,128)(2,1)S(1)}, u32[]{:S(2)}) copy-start(bf16[1,8,96,2048]{3,2,1,0:T(8,128)(2,1)S(1)} %get-tuple-element.24) | copy-start | bytes 9437188
  65.9 2.0 %copy-start.6 = (bf16[1,2048,256]{2,1,0:T(8,128)(2,1)S(1)}, bf16[1,2048,256]{2,1,0:T(8,128)(2,1)}, u32[]{:S(2)}) copy-start(bf16[1,2048,256]{2,1,0:T(8,128)(2,1)} %param.17) | copy-start | bytes 3145732
  67.9 4.1 %copy-start.19 = (f32[768,256]{1,0:T(8,128)}, f32[768,256]{1,0:T(8,128)S(1)}, u32[]{:S(2)}) copy-start(f32[768,256]{1,0:T(8,128)S(1)} %fusion.43) | copy-start | bytes 2359300
  67.9 2.0 %copy-start.18 = (bf16[1,256,2048]{2,1,0:T(8,128)(2,1)S(1)}, bf16[1,256,2048]{2,1,0:T(8,128)(2,1)}, u32[]{:S(2)}) copy-start(bf16[1,256,2048]{2,1,0:T(8,128)(2,1)} %param.18) | copy-start | bytes 3145732
  68.9 3.1 %copy-start.20 = (f32[768,256]{1,0:T(8,128)}, f32[768,256]{1,0:T(8,128)S(1)}, u32[]{:S(2)}) copy-start(f32[768,256]{1,0:T(8,128)S(1)} %fusion.45) | copy-start | bytes 2359300
  72.0 53.5 %copy-start.17 = (bf16[3,256]{1,0:T(4,128)(2,1)S(1)}, bf16[3,256]{1,0:T(4,128)(2,1)}, u32[]{:S(2)}) copy-start(bf16[3,256]{1,0:T(4,128)(2,1)} %param.22) | copy-start | bytes 4612
  72.0 53.5 %copy-start.13 = (f32[256,256]{1,0:T(8,128)S(1)}, f32[256,256]{1,0:T(8,128)}, u32[]{:S(2)}) copy-start(f32[256,256]{1,0:T(8,128)} %copy-done.12) | copy-start | bytes 786436
  72.0 53.5 %copy-start.16 = (bf16[256,256]{1,0:T(8,128)(2,1)S(1)}, bf16[256,256]{1,0:T(8,128)(2,1)}, u32[]{:S(2)}) copy-start(bf16[256,256]{1,0:T(8,128)(2,1)} %param.19) | copy-start | bytes 393220
  124.7 3.5 %copy-start.7 = (bf16[256,2048]{1,0:T(8,128)(2,1)S(1)}, bf16[256,2048]{1,0:T(8,128)(2,1)}, u32[]{:S(2)}) copy-start(bf16[256,2048]{1,0:T(8,128)(2,1)} %get-tuple-element.15) | copy-start | bytes 3145732
  161.7 4.5 %copy-start.2 = (bf16[1,8,96,2048]{3,2,1,0:T(8,128)(2,1)S(1)}, bf16[1,8,96,2048]{3,2,1,0:T(8,128)(2,1)}, u32[]{:S(2)}) copy-start(bf16[1,8,96,2048]{3,2,1,0:T(8,128)(2,1)} %copy-done.1) | copy-start | bytes 9437188
  161.7 4.5 %copy-start.11 = (bf16[768,256]{1,0:T(8,128)(2,1)S(1)}, bf16[768,256]{1,0:T(8,128)(2,1)}, u32[]{:S(2)}) copy-start(bf16[768,256]{1,0:T(8,128)(2,1)} %get-tuple-element.26) | copy-start | bytes 1179652
  166.2 2.0 %copy-start.10 = (bf16[768,256]{1,0:T(8,128)(2,1)S(1)}, bf16[768,256]{1,0:T(8,128)(2,1)}, u32[]{:S(2)}) copy-start(bf16[768,256]{1,0:T(8,128)(2,1)} %get-tuple-element.27) | copy-start | bytes 1179652
  168.2 2.0 %copy-start.15 = (f32[256,256]{1,0:T(8,128)S(1)}, f32[256,256]{1,0:T(8,128)}, u32[]{:S(2)}) copy-start(f32[256,256]{1,0:T(8,128)} %get-tuple-element.43) | copy-start | bytes 786436
  168.2 2.8 %copy-start.14 = (bf16[256,512]{1,0:T(8,128)(2,1)S(1)}, bf16[256,512]{1,0:T(8,128)(2,1)}, u32[]{:S(2)}) copy-start(bf16[256,512]{1,0:T(8,128)(2,1)} %get-tuple-element.44) | copy-start | bytes 786436

commit v2 on v1

v2 whole, which is shorter than its diff:
```python
import functools

import jax
import jax.numpy as jnp
from jax import lax
from jax.experimental import pallas as pl
from jax.experimental.pallas import tpu as pltpu
from jax.sharding import PartitionSpec as P

MESH = pl.DeviceIdType.MESH
BF16, F32 = jnp.bfloat16, jnp.float32
VMEM = pl.BlockSpec(memory_space=pltpu.VMEM)
ANY = pl.BlockSpec(memory_space=pl.ANY)


def coordinates(sp_size, tp_size):
    me, mine = lax.axis_index("sp"), lax.axis_index("tp")
    near = mine + 1 - 2 * (mine % 2)
    far = (mine + tp_size // 2) % tp_size
    return me, mine, near, far


def greet(sp_size, me, tp_partners):
    barrier = pltpu.get_barrier_semaphore()

    def one(i, carry):
        pl.semaphore_signal(
            barrier, inc=1, device_id={"sp": (me + 1 + i) % sp_size}, device_id_type=MESH
        )
        return carry

    lax.fori_loop(0, sp_size - 1, one, 0)
    for partner in tp_partners:
        pl.semaphore_signal(barrier, inc=1, device_id={"tp": partner}, device_id_type=MESH)
    pl.semaphore_wait(barrier, sp_size - 1 + len(tp_partners))


def remote(src, dst, send_sem, recv_sem, to):
    return pltpu.make_async_remote_copy(
        src_ref=src,
        dst_ref=dst,
        send_sem=send_sem,
        recv_sem=recv_sem,
        device_id=to,
        device_id_type=MESH,
    )


def each(count, body):
    def step(i, carry):
        body(i)
        return carry

    lax.fori_loop(0, count, step, 0)


def expert_kernel(
    sp_size,
    tp_size,
    send,
    own,
    tail,
    w_gate,
    w_up,
    w_down,
    place,
    cotangent,
    rows_h,
    rows_s,
    hid,
    d_pre,
    d_up,
    residual,
    full,
    earlier,
    rows,
    near_out,
    near_in,
    kept,
    far_out,
    far_in,
    back_out,
    back,
    total,
    row_sems,
    sems,
    save_sems,
    all_sems,
    own_sem,
    tail_sems,
):
    me, mine, near, far = coordinates(sp_size, tp_size)
    share = send.shape[3]
    near_far = (near + tp_size // 2) % tp_size
    last = sp_size - 1

    def columns(owner):
        return pl.ds(pl.multiple_of(owner * share, 128), share)

    def peer(i):
        return (me + sp_size - 1 - i) % sp_size

    keep = pltpu.make_async_copy(own, rows.at[:, me], own_sem)
    keep.start()
    greet(sp_size, me, (near, far))
    halo = remote(tail, earlier, tail_sems.at[0], tail_sems.at[1], {"sp": (me + 1) % sp_size})
    halo.start()

    def out(i):
        to = (me + 1 + i) % sp_size
        return remote(
            send.at[:, to],
            rows.at[:, me, :, columns(mine)],
            row_sems.at[0, i],
            row_sems.at[1, i],
            {"sp": to},
        )

    def onward(i, owner, lane, partner):
        block = rows.at[:, peer(i), :, columns(owner)]
        return remote(
            block, block, row_sems.at[2 * lane, i], row_sems.at[2 * lane + 1, i], {"tp": partner}
        )

    def save(i):
        which = peer(i)
        return (
            pltpu.make_async_copy(rows.at[0, which], rows_h.at[which], save_sems.at[0, i]),
            pltpu.make_async_copy(rows.at[1, which], rows_s.at[which], save_sems.at[1, i]),
        )

    def across(i):
        return remote(near_out.at[i], near_in.at[i], sems.at[0, i], sems.at[1, i], {"tp": near})

    def over(i):
        return remote(far_out.at[i], far_in.at[i], sems.at[2, i], sems.at[3, i], {"tp": far})

    def home(i):
        return remote(
            back_out.at[i], back.at[i], sems.at[4, i], sems.at[5, i], {"sp": peer(i)}
        )

    each(last, lambda i: out(i).start())

    def work(i):
        which = peer(i)
        for copy in save(i):
            copy.start()
        dims = (((1,), (1,)), ((), ()))
        row_h, row_s = rows[0, which], rows[1, which]
        pre_gate = jnp.dot(row_h, w_gate[...], preferred_element_type=F32)
        pre_up = jnp.dot(row_h, w_up[...], preferred_element_type=F32)
        d_hid = lax.dot_general(row_s, w_down[...], dims, preferred_element_type=F32)
        sigma = 1.0 / (1.0 + jnp.exp(-pre_gate))
        silu_gate = pre_gate * sigma
        up = (d_hid * silu_gate).astype(BF16)
        pre = (d_hid * pre_up * sigma * (1.0 + pre_gate * (1.0 - sigma))).astype(BF16)
        hid[which] = (silu_gate * pre_up).astype(BF16)
        d_up[which] = up
        d_pre[which] = pre

        def product(owner):
            return lax.dot_general(
                pre, w_gate[columns(owner), :], dims, preferred_element_type=F32
            ) + lax.dot_general(up, w_up[columns(owner), :], dims, preferred_element_type=F32)

        near_out[i, 0] = product(near).astype(BF16)
        near_out[i, 1] = product(near_far).astype(BF16)
        across(i).start()
        kept[i, 0] = product(mine)
        kept[i, 1] = product(far)

    def second(i):
        across(i).wait_recv()
        far_out[i] = (kept[i, 1] + near_in[i, 1].astype(F32)).astype(BF16)
        over(i).start()

    def summed(i):
        over(i).wait_recv()
        return (kept[i, 0] + near_in[i, 0].astype(F32) + far_in[i].astype(F32)).astype(BF16)

    def arrive(i):
        out(i).wait_recv()
        onward(i, mine, 1, far).start()
        onward(i, mine, 2, near).start()

    def cross(i):
        onward(i, mine, 1, far).wait_recv()
        onward(i, far, 3, near).start()

    def ready(i):
        onward(i, mine, 2, near).wait_recv()
        onward(i, far, 3, near).wait_recv()

    def third(i):
        back_out[i] = summed(i)
        home(i).start()

    def step(i):
        pl.when(i < last)(lambda: arrive(i))
        pl.when((i >= 1) & (i < last + 1))(lambda: cross(i - 1))
        pl.when((i >= 2) & (i < last + 2))(lambda: ready(i - 2))
        pl.when(i == 1)(keep.wait)
        pl.when((i >= 1) & (i < last + 2))(lambda: work((i + last - 1) % sp_size))
        pl.when((i >= 2) & (i < last + 3))(lambda: second((i + last - 2) % sp_size))
        pl.when((i >= 4) & (i < last + 4))(lambda: third(i - 4))

    each(last + 4, step)

    total[...] = cotangent[...].astype(F32) + jnp.dot(
        place[me], summed(last), preferred_element_type=F32
    )

    def collect(i):
        home(i).wait_recv()
        total[...] += jnp.dot(
            place[(me + 1 + i) % sp_size], back[i], preferred_element_type=F32
        )

    each(last, collect)
    result = total[...].astype(BF16)
    residual[...] = result
    full[:, columns(mine)] = result

    def gathered(owner, lane, partner):
        block = full.at[:, columns(owner)]
        return remote(block, block, all_sems.at[2 * lane], all_sems.at[2 * lane + 1], {"tp": partner})

    to_far, to_near = gathered(mine, 0, far), gathered(mine, 1, near)
    to_far.start()
    to_near.start()

    def finish(i):
        across(i).wait_send()
        over(i).wait_send()
        for copy in save(i):
            copy.wait()

    def finish_rows(i):
        out(i).wait_send()
        onward(i, mine, 1, far).wait_send()
        onward(i, mine, 2, near).wait_send()
        onward(i, far, 3, near).wait_send()
        home(i).wait_send()

    each(sp_size, finish)
    each(last, finish_rows)
    halo.wait()
    to_far.wait_recv()
    forward = gathered(far, 2, near)
    forward.start()
    to_far.wait_send()
    to_near.wait()
    forward.wait()


def reduce_kernel(sp_size, part, head, out, following, pair_in, pair_out, land, sems, head_sems):
    me = lax.axis_index("sp")
    side, pair, pairs = me % 2, me // 2, sp_size // 2
    greet(sp_size, me, ())
    halo = remote(
        head, following, head_sems.at[0], head_sems.at[1], {"sp": (me + sp_size - 1) % sp_size}
    )
    halo.start()

    def owner(i):
        return (pair + 1 + i) % pairs

    def beside(i):
        return remote(
            part.at[2 * owner(i) + 1 - side],
            pair_in.at[i],
            sems.at[0, i],
            sems.at[1, i],
            {"sp": me + 1 - 2 * side},
        )

    def along(i):
        return remote(
            pair_out.at[i], land.at[i], sems.at[2, i], sems.at[3, i], {"sp": 2 * owner(i) + side}
        )

    each(pairs, lambda i: beside(i).start())

    def both(i):
        beside(i).wait_recv()
        return part[2 * owner(i) + side].astype(F32) + pair_in[i].astype(F32)

    def onward(i):
        pair_out[i] = both(i).astype(BF16)
        along(i).start()

    each(pairs - 1, onward)
    out[...] = both(pairs - 1)

    def add(i):
        along(i).wait_recv()
        out[...] += land[i].astype(F32)

    each(pairs - 1, add)
    each(pairs, lambda i: beside(i).wait_send())
    each(pairs - 1, lambda i: along(i).wait_send())
    halo.wait()


def communicate(kernel, number, inputs, outputs, scratch, unplaced=0):
    return pl.pallas_call(
        kernel,
        out_shape=[jax.ShapeDtypeStruct(shape, kind) for shape, kind in outputs],
        in_specs=[VMEM] * len(inputs),
        out_specs=[ANY] * unplaced + [VMEM] * (len(outputs) - unplaced),
        scratch_shapes=scratch,
        compiler_params=pltpu.CompilerParams(collective_id=number, has_side_effects=True),
    )(*inputs)


def per_device(
    hidden_in,
    cotangent,
    routes,
    routing_weights,
    w_gate,
    w_up,
    w_down,
    b_gate,
    c_gate,
    x_in,
    taps,
    w_out,
):
    tok_rows, model_width = hidden_in.shape
    top_k = routes.shape[1]
    sp_size = lax.axis_size("sp")
    tp_size = lax.axis_size("tp")
    experts = w_gate.shape[0] * sp_size
    capacity = 3 * tok_rows * top_k // (2 * experts)
    share = model_width // tp_size
    channels = x_in.shape[1]
    offset = lax.axis_index("tp") * share
    me = lax.axis_index("sp")
    w_gate, w_up, w_down = w_gate[0], w_up[0], w_down[0]

    expert_ids = jnp.arange(experts, dtype=jnp.int32)
    hit = routes[:, :, None] == expert_ids[None, None, :]
    member = jnp.any(hit, axis=1)
    weight = jnp.sum(jnp.where(hit, routing_weights[:, :, None], 0.0), axis=1)
    lower = jnp.tri(tok_rows, k=-1, dtype=BF16)
    position = jnp.dot(lower, member.astype(BF16), preferred_element_type=F32).astype(jnp.int32)
    position = jnp.where(member, position, -1)
    slots = jnp.arange(capacity, dtype=jnp.int32)
    taken = position.T[:, None, :] == slots[None, :, None]
    select = taken.astype(BF16)
    place = (position.T[:, :, None] == slots[None, None, :]).astype(BF16)
    slot_weight = jnp.sum(jnp.where(taken, weight.T[:, None, :], 0.0), axis=2)

    def pick(chosen, weights, rows_src, cot_src):
        rows = jnp.einsum("...t,td->...d", chosen, rows_src, preferred_element_type=F32)
        cot = jnp.einsum("...t,td->...d", chosen, cot_src, preferred_element_type=F32)
        return jnp.stack([rows.astype(BF16), (weights[..., None] * cot).astype(BF16)])

    rows_src = lax.dynamic_slice_in_dim(hidden_in, offset, share, 1)
    cot_src = lax.dynamic_slice_in_dim(cotangent, offset, share, 1)
    send = pick(select, slot_weight, rows_src, cot_src)
    own = pick(select[me], slot_weight[me], hidden_in, cotangent)

    c_f, x_f, b_f = c_gate.astype(F32), x_in.astype(F32), b_gate.astype(F32)
    gated = c_f * x_f
    hidden = w_gate.shape[1]
    row_shape, hid_shape = (sp_size, capacity, model_width), (sp_size, capacity, hidden)
    rows_h, rows_s, hid, d_pre, d_up, residual_grad, full_grad, earlier = communicate(
        functools.partial(expert_kernel, sp_size, tp_size),
        0,
        (send, own, gated[tok_rows - 8 :], w_gate, w_up, w_down, place, cot_src),
        [(row_shape, BF16)] * 2
        + [(hid_shape, BF16)] * 3
        + [((tok_rows, share), BF16), ((tok_rows, model_width), BF16), ((8, channels), F32)],
        [
            pltpu.VMEM((2, sp_size, capacity, model_width), BF16),
            pltpu.VMEM((sp_size, 2, capacity, share), BF16),
            pltpu.VMEM((sp_size, 2, capacity, share), BF16),
            pltpu.VMEM((sp_size, 2, capacity, share), F32),
            pltpu.VMEM((sp_size, capacity, share), BF16),
            pltpu.VMEM((sp_size, capacity, share), BF16),
            pltpu.VMEM((sp_size - 1, capacity, share), BF16),
            pltpu.VMEM((sp_size - 1, capacity, share), BF16),
            pltpu.VMEM((tok_rows, share), F32),
            pltpu.SemaphoreType.DMA((8, sp_size - 1)),
            pltpu.SemaphoreType.DMA((6, sp_size)),
            pltpu.SemaphoreType.DMA((2, sp_size)),
            pltpu.SemaphoreType.DMA((6,)),
            pltpu.SemaphoreType.DMA,
            pltpu.SemaphoreType.DMA((2,)),
        ],
        unplaced=2,
    )
    flat = sp_size * capacity
    rows_h, rows_s = rows_h.reshape(flat, model_width), rows_s.reshape(flat, model_width)
    hid, d_pre, d_up = (a.reshape(flat, hidden) for a in (hid, d_pre, d_up))
    grad_down = jnp.einsum("rf,rd->fd", hid, rows_s, preferred_element_type=F32).astype(BF16)
    grad_gate = jnp.einsum("rd,rf->df", rows_h, d_pre, preferred_element_type=F32).astype(BF16)
    grad_up = jnp.einsum("rd,rf->df", rows_h, d_up, preferred_element_type=F32).astype(BF16)

    taps_f = taps.astype(F32)
    earlier = jnp.where(me == 0, 0.0, earlier[6:])
    padded = jnp.concatenate([earlier, gated], axis=0)
    conv = (
        taps_f[0] * padded[0:tok_rows]
        + taps_f[1] * padded[1 : tok_rows + 1]
        + taps_f[2] * padded[2 : tok_rows + 2]
    )
    y_short = (b_f * conv).astype(BF16)
    d_y = jnp.dot(full_grad, w_out, preferred_element_type=F32)
    grad_b = (d_y * conv).astype(BF16)
    d_conv = b_f * d_y
    part = jnp.einsum("td,tc->dc", full_grad, y_short, preferred_element_type=F32).astype(BF16)
    block = model_width // sp_size
    out_proj_grad, following = communicate(
        functools.partial(reduce_kernel, sp_size),
        1,
        (part.reshape(sp_size, block, channels), d_conv[:8]),
        [((block, channels), F32), ((8, channels), F32)],
        [
            pltpu.VMEM((sp_size // 2, block, channels), BF16),
            pltpu.VMEM((sp_size // 2, block, channels), BF16),
            pltpu.VMEM((sp_size // 2, block, channels), BF16),
            pltpu.SemaphoreType.DMA((4, sp_size // 2)),
            pltpu.SemaphoreType.DMA((2,)),
        ],
    )
    following = jnp.where(me == sp_size - 1, 0.0, following[:2])
    later = jnp.concatenate([d_conv, following], axis=0)
    d_v = (
        taps_f[2] * later[0:tok_rows]
        + taps_f[1] * later[1 : tok_rows + 1]
        + taps_f[0] * later[2 : tok_rows + 2]
    )
    grad_c = (d_v * x_f).astype(BF16)
    grad_x = (d_v * c_f).astype(BF16)
    grads = (grad_gate[None], grad_up[None], grad_down[None])
    return grads + (out_proj_grad, residual_grad, grad_b, grad_c, grad_x)


def solution(mesh):
    return jax.shard_map(
        per_device,
        mesh=mesh,
        in_specs=(
            P("sp", None),
            P("sp", None),
            P("sp", None),
            P("sp", None),
            P("sp", None, "tp"),
            P("sp", None, "tp"),
            P("sp", "tp", None),
            P("sp", "tp"),
            P("sp", "tp"),
            P("sp", "tp"),
            P(None, "tp"),
            P(None, "tp"),
        ),
        out_specs=(
            P("sp", None, "tp"),
            P("sp", None, "tp"),
            P("sp", "tp", None),
            P("sp", "tp"),
            P("sp", "tp"),
            P("sp", "tp"),
            P("sp", "tp"),
            P("sp", "tp"),
        ),
        check_vma=False,
    )
```

time: 172 us -> 146 us (0.85)
  Pallas kernels: 134 us -> 117 us
  local copies, waits for them, and re-layouts: 9.24 us -> 3.65 us
  matrix products: 19.6 us -> 15.1 us
    pallas_call x3 -> x2, Pallas kernels: 134 us -> 117 us  [communicate(): pl.pallas_call(kernel, out_shape=[jax.ShapeDtypeStruct(shape, kind) for s...]
    dot_general x3 -> x0, matrix products: 4.07 us -> none  [the longest x1 2.11 us: per_device(): d_hid = jnp.einsum('rd,fd->rf', rows_s, w_down, preferred_element_type=F32)]
    slice x1 -> x0, local copies, waits for them, and re-layouts: 3.5 us -> none  [per_device(): rows_s = rows[1].reshape(sp_size * capacity, model_width)]
    unnamed x44 -> x28, local copies, waits for them, and re-layouts: 3.48 us -> 1.47 us
where the time goes in v2:
time: 146 us; the launch traced here: 144 us
  Pallas kernels  117 us (80%)
  matrix products  15.1 us (10%)
  other arithmetic  8.17 us (6%)
  local copies, waits for them, and re-layouts  3.65 us (2%)
    pallas_call x2, Pallas kernels, communicate(): pl.pallas_call(kernel, out_shape=[jax.ShapeDtypeStruct(shape, kind) for s...  117 us
    dot_general x1, matrix products, per_device(): jnp.einsum('rf,rd->fd', hid, rows_s, preferred_element_type=F32)  4.01 us

profile of v2, /device:TPU:15, one launch (start us, length us, event | category | flops | bytes accessed | tf_op | source)
XLA Modules:
  0.0 144.3 jit_solution(8641858421008284768)
XLA Ops:
  0.6 0.0 copy-start
  0.7 0.8 fusion.37
  1.4 0.2 fusion.11
  1.7 0.7 select_reduce_fusion.1
  2.4 0.2 select_reduce_fusion
  2.6 0.1 iota_compare_fusion.1
  2.8 1.5 %fusion.8 = bf16[1,96,2048]{2,1,0:T(8,128)(2,1)S(1)} fusion(bf16[256,2048]{1,0:T(8,128)(2,1)} %param.13, f32[96]{0:T(128)S(1)} %fusion.41, pred[8,96,256]{2,1,0:T(32,128)(4,1)S(1)} %iota_compare_fusion.1, s32[]{:T(128)S(6)} %select_n.39), kind=kOutput, calls=%fused_computation.14 | convolution fusion | flops 101056512 | bytes 1466884 | tf_op jit(solution)/shard_map/...t,td->...d/dot_general | solution.py:358
  4.3 0.3 fusion.7
  4.6 1.0 pad_maximum_fusion.1.own
  5.6 1.0 constant_dynamic-slice_fusion.1.cotangent
  6.5 0.0 copy-start.1
  6.6 0.4 fusion.10
  6.9 0.4 fusion.9
  7.3 0.0 copy-start.3
  7.3 0.0 copy-start.4
  7.4 1.3 pad_maximum_fusion.send
  8.6 1.1 fusion.12.place
  9.8 0.6 slice.47.tail
  10.4 83.7 %shard_map.179 = (bf16[8,96,2048]{2,1,0:T(8,128)(2,1)}, bf16[8,96,2048]{2,1,0:T(8,128)(2,1)}, bf16[8,96,256]{2,1,0:T(8,128)(2,1)}, bf16[8,96,256]{2,1,0:T(8,128)...) custom-call(bf16[2,8,96,512]{3,2,1,0:T(8,128)(2,1)} %pad_maximum_fus, ...), custom_call_target="tpu_custom_call" | custom-call | tf_op jit(solution)/shard_map/pallas_call | solution.py:307
  94.1 0.8 slice_select_fusion.1
  94.9 2.6 %multiply_convert_fusion.1 = (bf16[256,256]{1,0:T(8,128)(2,1)}, f32[256,256]{1,0:T(8,128)S(1)}, f32[256,256]{1,0:T(8,128)S(1)}) fusion(f32[256,256]{1,0:T(8,128)S(1)} %convert_multiply_fusion.3, f32[256]{0:T(256)S(1)} %bitcast.76, f32[2,256]{1,0:T(2,128)S(1)} %slice_select_fusion.1, f32[256]{0:T(256)S(1)} %bitcast.74, f32[256]{0:T(256)S(1)} %bitcast.72, ...), kind=kOutput, calls=%fused_computation.55 | convolution fusion | flops 269156352 | bytes 3150848 | tf_op jit(solution)/shard_map/dot_general | solution.py:412
  97.6 1.5 %convolution_convert_fusion = bf16[2048,256]{1,0:T(8,128)(2,1)} fusion(bf16[256,2048]{1,0:T(8,128)(2,1)S(1)} %copy-done.2, f32[256,256]{1,0:T(8,128)S(1)} %get-tuple-element.31, bf16[256,256]{1,0:T(8,128)(2,1)S(1)} %copy-done.7), kind=kOutput, calls=%fused_computation.3 | convolution fusion | flops 269156352 | bytes 2490368 | tf_op jit(solution)/shard_map/td,tc->dc/dot_general | solution.py:415
  99.0 0.6 slice.53.head
  99.6 33.0 %shard_map.180 = (f32[256,256]{1,0:T(8,128)}, f32[8,256]{1,0:T(8,128)}) custom-call(bf16[8,256,256]{2,1,0:T(8,128)(2,1)} %bitcast.67, f32[8,256]{1,0:T(8,128)} %slice.53.head), custom_call_target="tpu_custom_call" | custom-call | tf_op jit(solution)/shard_map/pallas_call | solution.py:307
  132.7 0.7 slice_select_fusion
  133.4 0.8 fusion.23
  134.1 0.7 fusion.24
  134.8 4.0 %fusion.3 = bf16[1,256,2048]{2,1,0:T(8,128)(2,1)} fusion(bf16[8,96,256]{2,1,0:T(8,128)(2,1)S(1)} %copy-done.12, bf16[8,96,2048]{2,1,0:T(8,128)(2,1)} %get-tuple-element.22), kind=kOutput, calls=%fused_computation.7 | convolution fusion | flops 805830656 | bytes 4587520 | tf_op jit(solution)/shard_map/rf,rd->fd/dot_general | solution.py:399
  138.9 2.0 %fusion.4 = bf16[1,2048,256]{2,1,0:T(8,128)(2,1)} fusion(bf16[8,96,2048]{2,1,0:T(8,128)(2,1)S(1)} %copy-done.9, bf16[8,96,256]{2,1,0:T(8,128)(2,1)S(1)} %copy-done.11), kind=kOutput, calls=%fused_computation.8 | convolution fusion | flops 805830656 | bytes 4587520 | tf_op jit(solution)/shard_map/rd,rf->df/dot_general | solution.py:401
  140.9 2.0 %fusion.5 = bf16[1,2048,256]{2,1,0:T(8,128)(2,1)} fusion(bf16[8,96,2048]{2,1,0:T(8,128)(2,1)S(1)} %copy-done.9, bf16[8,96,256]{2,1,0:T(8,128)(2,1)S(1)} %copy-done.10), kind=kOutput, calls=%fused_computation.9 | convolution fusion | flops 805830656 | bytes 4587520 | tf_op jit(solution)/shard_map/rd,rf->df/dot_general | solution.py:400
  142.9 0.7 copy.27
  143.6 0.7 copy.28
  (26 shorter events, 0.1 us)
Async XLA Ops:
  0.6 3.7 %copy-start = (bf16[256,2048]{1,0:T(8,128)(2,1)S(1)}, bf16[256,2048]{1,0:T(8,128)(2,1)}, u32[]{:S(2)}) copy-start(bf16[256,2048]{1,0:T(8,128)(2,1)} %param.12) | copy-start | bytes 3145732
  6.5 2.1 %copy-start.1 = (bf16[256,512]{1,0:T(8,128)(2,1)}, bf16[256,512]{1,0:T(8,128)(2,1)S(1)}, u32[]{:S(2)}) copy-start(bf16[256,512]{1,0:T(8,128)(2,1)S(1)} %constant_dynamic-slice_fusion.1.cotangent) | copy-start | bytes 786436
  7.3 2.4 %copy-start.3 = (bf16[256,256]{1,0:T(8,128)(2,1)S(1)}, bf16[256,256]{1,0:T(8,128)(2,1)}, u32[]{:S(2)}) copy-start(bf16[256,256]{1,0:T(8,128)(2,1)} %param.20) | copy-start | bytes 393220
  7.3 2.4 %copy-start.4 = (bf16[256,256]{1,0:T(8,128)(2,1)S(1)}, bf16[256,256]{1,0:T(8,128)(2,1)}, u32[]{:S(2)}) copy-start(bf16[256,256]{1,0:T(8,128)(2,1)} %param.21) | copy-start | bytes 393220
  10.4 84.5 %copy-start.8 = (bf16[3,256]{1,0:T(4,128)(2,1)S(1)}, bf16[3,256]{1,0:T(4,128)(2,1)}, u32[]{:S(2)}) copy-start(bf16[3,256]{1,0:T(4,128)(2,1)} %param.22) | copy-start | bytes 4612
  10.4 84.5 %copy-start.7 = (bf16[256,256]{1,0:T(8,128)(2,1)S(1)}, bf16[256,256]{1,0:T(8,128)(2,1)}, u32[]{:S(2)}) copy-start(bf16[256,256]{1,0:T(8,128)(2,1)} %param.19) | copy-start | bytes 393220
  94.1 3.5 %copy-start.2 = (bf16[256,2048]{1,0:T(8,128)(2,1)S(1)}, bf16[256,2048]{1,0:T(8,128)(2,1)}, u32[]{:S(2)}) copy-start(bf16[256,2048]{1,0:T(8,128)(2,1)} %get-tuple-element.23) | copy-start | bytes 3145732
  97.6 37.3 %copy-start.12 = (bf16[8,96,256]{2,1,0:T(8,128)(2,1)S(1)}, bf16[8,96,256]{2,1,0:T(8,128)(2,1)}, u32[]{:S(2)}) copy-start(bf16[8,96,256]{2,1,0:T(8,128)(2,1)} %get-tuple-element.21) | copy-start | bytes 1179652
  134.8 4.0 %copy-start.9 = (bf16[8,96,2048]{2,1,0:T(8,128)(2,1)S(1)}, bf16[8,96,2048]{2,1,0:T(8,128)(2,1)}, u32[]{:S(2)}) copy-start(bf16[8,96,2048]{2,1,0:T(8,128)(2,1)} %get-tuple-element.18) | copy-start | bytes 9437188
  134.8 4.0 %copy-start.11 = (bf16[8,96,256]{2,1,0:T(8,128)(2,1)S(1)}, bf16[8,96,256]{2,1,0:T(8,128)(2,1)}, u32[]{:S(2)}) copy-start(bf16[8,96,256]{2,1,0:T(8,128)(2,1)} %get-tuple-element.20) | copy-start | bytes 1179652
  138.8 2.0 %copy-start.10 = (bf16[8,96,256]{2,1,0:T(8,128)(2,1)S(1)}, bf16[8,96,256]{2,1,0:T(8,128)(2,1)}, u32[]{:S(2)}) copy-start(bf16[8,96,256]{2,1,0:T(8,128)(2,1)} %get-tuple-element.19) | copy-start | bytes 1179652
  140.9 2.0 %copy-start.6 = (f32[256,256]{1,0:T(8,128)S(1)}, f32[256,256]{1,0:T(8,128)}, u32[]{:S(2)}) copy-start(f32[256,256]{1,0:T(8,128)} %get-tuple-element.47) | copy-start | bytes 786436
  140.9 2.8 %copy-start.5 = (bf16[256,512]{1,0:T(8,128)(2,1)S(1)}, bf16[256,512]{1,0:T(8,128)(2,1)}, u32[]{:S(2)}) copy-start(bf16[256,512]{1,0:T(8,128)(2,1)} %get-tuple-element.48) | copy-start | bytes 786436

commit v3 on v2

--- a/solution.py
+++ b/solution.py
@@ -98,7 +98,12 @@
         return pl.ds(pl.multiple_of(owner * share, 128), share)
 
     def peer(i):
-        return (me + sp_size - 1 - i) % sp_size
+        mask = ((i + 1) * 3) % sp_size
+        other, bit = me, 1
+        while bit < sp_size:
+            other = other + ((mask // bit) % 2) * bit * (1 - 2 * ((me // bit) % 2))
+            bit *= 2
+        return other
 
     keep = pltpu.make_async_copy(own, rows.at[:, me], own_sem)
     keep.start()
@@ -107,7 +112,7 @@
     halo.start()
 
     def out(i):
-        to = (me + 1 + i) % sp_size
+        to = peer(i)
         return remote(
             send.at[:, to],
             rows.at[:, me, :, columns(mine)],
@@ -214,7 +219,7 @@
     def collect(i):
         home(i).wait_recv()
         total[...] += jnp.dot(
-            place[(me + 1 + i) % sp_size], back[i], preferred_element_type=F32
+            place[peer(i)], back[i], preferred_element_type=F32
         )
 
     each(last, collect)

time: 146 us -> 137 us (0.938)
  Pallas kernels: 117 us -> 108 us
    pallas_call x2, Pallas kernels: 117 us -> 108 us  [communicate(): pl.pallas_call(kernel, out_shape=[jax.ShapeDtypeStruct(shape, kind) for s...]
where the time goes in v3:
time: 137 us; the launch traced here: 135 us
  Pallas kernels  108 us (79%)
  matrix products  15.1 us (11%)
  other arithmetic  8.17 us (6%)
  local copies, waits for them, and re-layouts  3.65 us (3%)
    pallas_call x2, Pallas kernels, communicate(): pl.pallas_call(kernel, out_shape=[jax.ShapeDtypeStruct(shape, kind) for s...  108 us
    dot_general x1, matrix products, per_device(): jnp.einsum('rf,rd->fd', hid, rows_s, preferred_element_type=F32)  4.01 us

profile of v3, /device:TPU:15, one launch (start us, length us, event | category | flops | bytes accessed | tf_op | source)
XLA Modules:
  0.0 135.2 jit_solution(2090610497756721919)
XLA Ops:
  0.6 0.0 copy-start
  0.7 0.8 fusion.37
  1.4 0.2 fusion.11
  1.7 0.7 select_reduce_fusion.1
  2.4 0.2 select_reduce_fusion
  2.6 0.1 iota_compare_fusion.1
  2.8 1.5 %fusion.8 = bf16[1,96,2048]{2,1,0:T(8,128)(2,1)S(1)} fusion(bf16[256,2048]{1,0:T(8,128)(2,1)} %param.13, f32[96]{0:T(128)S(1)} %fusion.41, pred[8,96,256]{2,1,0:T(32,128)(4,1)S(1)} %iota_compare_fusion.1, s32[]{:T(128)S(6)} %select_n.39), kind=kOutput, calls=%fused_computation.14 | convolution fusion | flops 101056512 | bytes 1466884 | tf_op jit(solution)/shard_map/...t,td->...d/dot_general | solution.py:363
  4.3 0.3 fusion.7
  4.6 1.0 pad_maximum_fusion.1.own
  5.6 1.0 constant_dynamic-slice_fusion.1.cotangent
  6.5 0.0 copy-start.1
  6.6 0.4 fusion.10
  6.9 0.4 fusion.9
  7.3 0.0 copy-start.3
  7.3 0.0 copy-start.4
  7.4 1.3 pad_maximum_fusion.send
  8.6 1.1 fusion.12.place
  9.8 0.6 slice.47.tail
  10.4 83.5 %shard_map.179 = (bf16[8,96,2048]{2,1,0:T(8,128)(2,1)}, bf16[8,96,2048]{2,1,0:T(8,128)(2,1)}, bf16[8,96,256]{2,1,0:T(8,128)(2,1)}, bf16[8,96,256]{2,1,0:T(8,128)...) custom-call(bf16[2,8,96,512]{3,2,1,0:T(8,128)(2,1)} %pad_maximum_fus, ...), custom_call_target="tpu_custom_call" | custom-call | tf_op jit(solution)/shard_map/pallas_call | solution.py:312
  93.9 0.8 slice_select_fusion.1
  94.7 2.6 %multiply_convert_fusion.1 = (bf16[256,256]{1,0:T(8,128)(2,1)}, f32[256,256]{1,0:T(8,128)S(1)}, f32[256,256]{1,0:T(8,128)S(1)}) fusion(f32[256,256]{1,0:T(8,128)S(1)} %convert_multiply_fusion.3, f32[256]{0:T(256)S(1)} %bitcast.76, f32[2,256]{1,0:T(2,128)S(1)} %slice_select_fusion.1, f32[256]{0:T(256)S(1)} %bitcast.74, f32[256]{0:T(256)S(1)} %bitcast.72, ...), kind=kOutput, calls=%fused_computation.55 | convolution fusion | flops 269156352 | bytes 3150848 | tf_op jit(solution)/shard_map/dot_general | solution.py:417
  97.3 1.5 %convolution_convert_fusion = bf16[2048,256]{1,0:T(8,128)(2,1)} fusion(bf16[256,2048]{1,0:T(8,128)(2,1)S(1)} %copy-done.2, f32[256,256]{1,0:T(8,128)S(1)} %get-tuple-element.31, bf16[256,256]{1,0:T(8,128)(2,1)S(1)} %copy-done.7), kind=kOutput, calls=%fused_computation.3 | convolution fusion | flops 269156352 | bytes 2490368 | tf_op jit(solution)/shard_map/td,tc->dc/dot_general | solution.py:420
  98.8 0.6 slice.53.head
  99.4 24.1 %shard_map.180 = (f32[256,256]{1,0:T(8,128)}, f32[8,256]{1,0:T(8,128)}) custom-call(bf16[8,256,256]{2,1,0:T(8,128)(2,1)} %bitcast.67, f32[8,256]{1,0:T(8,128)} %slice.53.head), custom_call_target="tpu_custom_call" | custom-call | tf_op jit(solution)/shard_map/pallas_call | solution.py:312
  123.6 0.7 slice_select_fusion
  124.3 0.8 fusion.23
  125.0 0.7 fusion.24
  125.7 4.0 %fusion.3 = bf16[1,256,2048]{2,1,0:T(8,128)(2,1)} fusion(bf16[8,96,256]{2,1,0:T(8,128)(2,1)S(1)} %copy-done.12, bf16[8,96,2048]{2,1,0:T(8,128)(2,1)} %get-tuple-element.22), kind=kOutput, calls=%fused_computation.7 | convolution fusion | flops 805830656 | bytes 4587520 | tf_op jit(solution)/shard_map/rf,rd->fd/dot_general | solution.py:404
  129.7 2.0 %fusion.4 = bf16[1,2048,256]{2,1,0:T(8,128)(2,1)} fusion(bf16[8,96,2048]{2,1,0:T(8,128)(2,1)S(1)} %copy-done.9, bf16[8,96,256]{2,1,0:T(8,128)(2,1)S(1)} %copy-done.11), kind=kOutput, calls=%fused_computation.8 | convolution fusion | flops 805830656 | bytes 4587520 | tf_op jit(solution)/shard_map/rd,rf->df/dot_general | solution.py:406
  131.8 2.0 %fusion.5 = bf16[1,2048,256]{2,1,0:T(8,128)(2,1)} fusion(bf16[8,96,2048]{2,1,0:T(8,128)(2,1)S(1)} %copy-done.9, bf16[8,96,256]{2,1,0:T(8,128)(2,1)S(1)} %copy-done.10), kind=kOutput, calls=%fused_computation.9 | convolution fusion | flops 805830656 | bytes 4587520 | tf_op jit(solution)/shard_map/rd,rf->df/dot_general | solution.py:405
  133.8 0.7 copy.27
  134.5 0.7 copy.28
  (26 shorter events, 0.1 us)
Async XLA Ops:
  0.6 3.7 %copy-start = (bf16[256,2048]{1,0:T(8,128)(2,1)S(1)}, bf16[256,2048]{1,0:T(8,128)(2,1)}, u32[]{:S(2)}) copy-start(bf16[256,2048]{1,0:T(8,128)(2,1)} %param.12) | copy-start | bytes 3145732
  6.5 2.1 %copy-start.1 = (bf16[256,512]{1,0:T(8,128)(2,1)}, bf16[256,512]{1,0:T(8,128)(2,1)S(1)}, u32[]{:S(2)}) copy-start(bf16[256,512]{1,0:T(8,128)(2,1)S(1)} %constant_dynamic-slice_fusion.1.cotangent) | copy-start | bytes 786436
  7.3 2.4 %copy-start.3 = (bf16[256,256]{1,0:T(8,128)(2,1)S(1)}, bf16[256,256]{1,0:T(8,128)(2,1)}, u32[]{:S(2)}) copy-start(bf16[256,256]{1,0:T(8,128)(2,1)} %param.20) | copy-start | bytes 393220
  7.3 2.4 %copy-start.4 = (bf16[256,256]{1,0:T(8,128)(2,1)S(1)}, bf16[256,256]{1,0:T(8,128)(2,1)}, u32[]{:S(2)}) copy-start(bf16[256,256]{1,0:T(8,128)(2,1)} %param.21) | copy-start | bytes 393220
  10.4 84.3 %copy-start.8 = (bf16[3,256]{1,0:T(4,128)(2,1)S(1)}, bf16[3,256]{1,0:T(4,128)(2,1)}, u32[]{:S(2)}) copy-start(bf16[3,256]{1,0:T(4,128)(2,1)} %param.22) | copy-start | bytes 4612
  10.4 84.3 %copy-start.7 = (bf16[256,256]{1,0:T(8,128)(2,1)S(1)}, bf16[256,256]{1,0:T(8,128)(2,1)}, u32[]{:S(2)}) copy-start(bf16[256,256]{1,0:T(8,128)(2,1)} %param.19) | copy-start | bytes 393220
  93.9 3.5 %copy-start.2 = (bf16[256,2048]{1,0:T(8,128)(2,1)S(1)}, bf16[256,2048]{1,0:T(8,128)(2,1)}, u32[]{:S(2)}) copy-start(bf16[256,2048]{1,0:T(8,128)(2,1)} %get-tuple-element.23) | copy-start | bytes 3145732
  97.3 28.4 %copy-start.12 = (bf16[8,96,256]{2,1,0:T(8,128)(2,1)S(1)}, bf16[8,96,256]{2,1,0:T(8,128)(2,1)}, u32[]{:S(2)}) copy-start(bf16[8,96,256]{2,1,0:T(8,128)(2,1)} %get-tuple-element.21) | copy-start | bytes 1179652
  125.7 4.0 %copy-start.9 = (bf16[8,96,2048]{2,1,0:T(8,128)(2,1)S(1)}, bf16[8,96,2048]{2,1,0:T(8,128)(2,1)}, u32[]{:S(2)}) copy-start(bf16[8,96,2048]{2,1,0:T(8,128)(2,1)} %get-tuple-element.18) | copy-start | bytes 9437188
  125.7 4.0 %copy-start.11 = (bf16[8,96,256]{2,1,0:T(8,128)(2,1)S(1)}, bf16[8,96,256]{2,1,0:T(8,128)(2,1)}, u32[]{:S(2)}) copy-start(bf16[8,96,256]{2,1,0:T(8,128)(2,1)} %get-tuple-element.20) | copy-start | bytes 1179652
  129.7 2.0 %copy-start.10 = (bf16[8,96,256]{2,1,0:T(8,128)(2,1)S(1)}, bf16[8,96,256]{2,1,0:T(8,128)(2,1)}, u32[]{:S(2)}) copy-start(bf16[8,96,256]{2,1,0:T(8,128)(2,1)} %get-tuple-element.19) | copy-start | bytes 1179652
  131.8 2.1 %copy-start.6 = (f32[256,256]{1,0:T(8,128)S(1)}, f32[256,256]{1,0:T(8,128)}, u32[]{:S(2)}) copy-start(f32[256,256]{1,0:T(8,128)} %get-tuple-element.47) | copy-start | bytes 786436
  131.8 2.8 %copy-start.5 = (bf16[256,512]{1,0:T(8,128)(2,1)S(1)}, bf16[256,512]{1,0:T(8,128)(2,1)}, u32[]{:S(2)}) copy-start(bf16[256,512]{1,0:T(8,128)(2,1)} %get-tuple-element.48) | copy-start | bytes 786436
